TPU v7x, 256 devices: a whole 4x4x8 slice. The times are simulated.
256 devices in a mesh: sp: 16 (over y, x), tp: 16 (over z, core).
Axes of the slice: x: 4, y: 4, z: 8, core: 2. Of those that a mesh axis runs over, the one named last changes fastest.
Arguments:
- queries: bfloat16 [16384, 1536], P('sp', 'tp'), may hold values from -34 to 34
- latent: bfloat16 [16384, 512], P('sp'), may hold values from -6 to 6
- rot_key: bfloat16 [16384, 32], P('sp'), may hold values from -34 to 34
- latent_gain: float32 [512], replicated, may hold values from 0.1 to 1.9
- key_up: bfloat16 [512, 1024], P(None, 'tp'), may hold values from -0.25 to 0.25
- value_up: bfloat16 [512, 1024], P(None, 'tp'), may hold values from -0.70710678 to 0.70710678
- query_gain: float32 [96], replicated, may hold values from 0.5 to 6
- key_gain: float32 [96], replicated, may hold values from 0.5 to 6
- out_gain: float32 [1024], replicated, may hold values from 0.1 to 1.9
- out_weight: bfloat16 [1024, 2048], replicated, may hold values from -0.1875 to 0.1875
- residual: bfloat16 [16384, 2048], P(('sp', 'tp')), may hold values from -6 to 6
- ffn_gain: float32 [2048], replicated, may hold values from 0.1 to 1.9
- routes: int32 [16384, 2], P(('sp', 'tp')), may hold values from 0 to 15, all different within a row; in each aligned block of 64 rows (0 to 63, 64 to 127, ...) at most 9 rows name the same one
- route_weights: float32 [16384, 2], P(('sp', 'tp')), may hold values from 0.2 to 1
- expert_gate: bfloat16 [16, 2048, 2048], P('sp', None, 'tp'), may hold values from -0.125 to 0.125
- expert_up: bfloat16 [16, 2048, 2048], P('sp', None, 'tp'), may hold values from -0.125 to 0.125
- expert_down: bfloat16 [16, 2048, 2048], P('sp', 'tp'), may hold values from -0.125 to 0.125
Outputs:
- layer_out: bfloat16 [16384, 2048], P(('sp', 'tp'))
Inputs may be any that keep to these rules, and one draw needn't show every extreme that they name: `routes`: the 2 experts of a token differ. Among the 64 rows of one device each expert is named by at most 9 rows, a bound that some block reaches.
All inputs are finite; a program needn't handle non-finite values.
Results may differ from a plain program's by a relative error of at most 0.02.
The roundings to bfloat16 on the way count: a program that leaves them out, or rounds other values in their place, can miss the bound.
Values may be sent and summed in bfloat16 or wider, within the bound.
A program may use at most 128 MiB of HBM per device.

v0:
```python
import jax
import jax.numpy as jnp
from jax import lax
from jax.sharding import PartitionSpec as P

D = 2048
NOPE = 64
ROPE = 32
VH = 64
TOPK = 2
QK = 96
epsilon = 1e-06
rope_base = 10000.0


def rms_scale(values):
    return lax.rsqrt(jnp.mean(values * values, axis=-1, keepdims=True) + epsilon)


def rotate_half(values, angles):
    half_dims = values.shape[-1] // 2
    first_half = values[..., :half_dims]
    second_half = values[..., half_dims:]
    cosine = jnp.cos(angles)
    sine_val = jnp.sin(angles)
    return jnp.concatenate(
        [
            first_half * cosine - second_half * sine_val,
            second_half * cosine + first_half * sine_val,
        ],
        axis=-1,
    )


def head_prepare(raw_rows, gain_vec, angles):
    normed_rows = raw_rows * rms_scale(raw_rows) * gain_vec
    turned_rows = rotate_half(normed_rows[..., NOPE:], angles[:, None, :])
    return jnp.concatenate([normed_rows[..., :NOPE], turned_rows], axis=-1).astype(jnp.bfloat16)


def slot_targets(route_rows, expert_total, slot_cap):
    flat_routes = route_rows.reshape(-1)
    one_hot = (flat_routes[:, None] == jnp.arange(expert_total, dtype=jnp.int32)[None, :]).astype(
        jnp.int32
    )
    earlier = jnp.cumsum(one_hot, axis=0) - one_hot
    rank_in = jnp.sum(earlier * one_hot, axis=1)
    return (flat_routes * slot_cap + rank_in).reshape(route_rows.shape)


def select_matrix(targets, slot_total):
    hits = targets[:, :, None] == jnp.arange(slot_total, dtype=jnp.int32)[None, None, :]
    return jnp.sum(hits.astype(jnp.bfloat16), axis=1)


def shards(
    queries,
    latent,
    rot_key,
    latent_gain,
    key_up,
    value_up,
    query_gain,
    key_gain,
    out_gain,
    out_weight,
    residual,
    ffn_gain,
    routes,
    route_weights,
    expert_gate,
    expert_up,
    expert_down,
):
    shard_len = queries.shape[0]
    local_heads = key_up.shape[1] // NOPE
    sp_count = lax.axis_size("sp")
    tp_count = lax.axis_size("tp")
    my_first = lax.axis_index("sp") * shard_len
    my_last = my_first + shard_len - 1
    positions = my_first + jnp.arange(shard_len, dtype=jnp.int32)
    inverse = rope_base ** (-jnp.arange(0, ROPE, 2, dtype=jnp.float32) / ROPE)
    angles = positions.astype(jnp.float32)[:, None] * inverse[None, :]
    lat_f32 = latent.astype(jnp.float32)
    normed_latent = (lat_f32 * rms_scale(lat_f32) * latent_gain).astype(jnp.bfloat16)
    key_nope = jnp.dot(normed_latent, key_up, preferred_element_type=jnp.float32).astype(
        jnp.bfloat16
    )
    value_rows = jnp.dot(normed_latent, value_up, preferred_element_type=jnp.float32).astype(
        jnp.bfloat16
    )
    shared = rot_key.astype(jnp.float32)[:, None, :]
    raw_keys = jnp.concatenate(
        [key_nope.astype(jnp.float32).reshape(shard_len, local_heads, NOPE), shared], axis=-1
    )
    key_rows = head_prepare(raw_keys, key_gain, angles)
    query_rows = head_prepare(
        queries.astype(jnp.float32).reshape(shard_len, local_heads, QK), query_gain, angles
    )
    query_heads = jnp.transpose(query_rows, (1, 0, 2))
    bundle = jnp.concatenate(
        [
            jnp.transpose(key_rows, (1, 2, 0)),
            jnp.transpose(value_rows.reshape(shard_len, local_heads, VH), (1, 2, 0)),
        ],
        axis=1,
    )
    score_scale = QK ** (-0.5)
    init_state = (
        jnp.full((local_heads, shard_len), -1e30, jnp.float32),
        jnp.zeros((local_heads, shard_len), jnp.float32),
        jnp.zeros((local_heads, shard_len, VH), jnp.float32),
    )
    key_piece = lax.all_gather(bundle, "sp", axis=2, tiled=True)
    block_count = key_piece.shape[2] // shard_len

    def one_block(block_index, running_state):
        first_key = block_index * shard_len

        def compute(inner):
            row_peak, row_total, weighted = inner
            key_part = lax.dynamic_slice_in_dim(key_piece, block_index * shard_len, shard_len, 2)
            scores = (
                jnp.einsum(
                    "hqc,hck->hqk",
                    query_heads,
                    key_part[:, :QK, :],
                    preferred_element_type=jnp.float32,
                )
                * score_scale
            )
            key_pos = first_key + jnp.arange(shard_len, dtype=jnp.int32)
            allowed = key_pos[None, None, :] <= positions[None, :, None]
            scores = jnp.where(allowed, scores, -1e30)
            new_peak = jnp.maximum(row_peak, jnp.max(scores, axis=2))
            exponent = jnp.where(allowed, jnp.exp(scores - new_peak[..., None]), 0.0)
            factor = jnp.exp(row_peak - new_peak)
            new_total = row_total * factor + jnp.sum(exponent, axis=2)
            contrib = jnp.einsum(
                "hqk,hvk->hqv",
                exponent.astype(jnp.bfloat16),
                key_part[:, QK:, :],
                preferred_element_type=jnp.float32,
            )
            return (new_peak, new_total, weighted * factor[..., None] + contrib)

        return lax.cond(first_key <= my_last, compute, lambda inner: inner, running_state)

    row_peak, row_total, weighted = lax.fori_loop(0, block_count, one_block, init_state)
    attended = (weighted / row_total[..., None]).astype(jnp.bfloat16)
    tok_count = residual.shape[0]
    head_major = jnp.transpose(attended, (1, 0, 2)).reshape(shard_len, local_heads * VH)
    token_rows = lax.all_to_all(head_major, "tp", split_axis=0, concat_axis=1, tiled=True).astype(
        jnp.float32
    )
    normed_rows = (token_rows * rms_scale(token_rows) * out_gain).astype(jnp.bfloat16)
    partials = jnp.einsum(
        "tgc,gcd->tgd",
        normed_rows.reshape(tok_count, tp_count, -1),
        out_weight.reshape(tp_count, -1, D),
        preferred_element_type=jnp.float32,
    )
    rounded = lax.optimization_barrier(partials.astype(jnp.bfloat16))
    mixed = jnp.sum(rounded.astype(jnp.float32), axis=1)
    middle = residual.astype(jnp.float32) + mixed
    ffn_input = (middle * rms_scale(middle) * ffn_gain).astype(jnp.bfloat16)
    slot_cap = max(2, 9 * tok_count * TOPK // (8 * sp_count))
    slot_total = sp_count * slot_cap
    targets = slot_targets(routes, sp_count, slot_cap)
    chooser = select_matrix(targets, slot_total)
    outbound = (
        jnp.einsum("ts,td->sd", chooser, ffn_input, preferred_element_type=jnp.float32)
        .astype(jnp.bfloat16)
        .reshape(sp_count, slot_cap, D)
    )
    arrived = lax.all_to_all(outbound, "sp", split_axis=0, concat_axis=0, tiled=True)
    item_count = arrived.shape[1]
    flat_rows = arrived.reshape(sp_count * item_count, D)
    row_block = lax.all_gather(flat_rows, "tp", axis=0, tiled=True)
    gate_pre = jnp.dot(row_block, expert_gate[0], preferred_element_type=jnp.float32)
    up_pre = jnp.dot(row_block, expert_up[0], preferred_element_type=jnp.float32)
    hidden = (jax.nn.silu(gate_pre) * up_pre).astype(jnp.bfloat16)
    served = lax.psum_scatter(
        jnp.dot(hidden, expert_down[0], preferred_element_type=jnp.float32).astype(jnp.bfloat16),
        "tp",
        scatter_dimension=0,
        tiled=True,
    ).reshape(sp_count, item_count, D)
    returned_rows = lax.all_to_all(served, "sp", split_axis=0, concat_axis=0, tiled=True).reshape(
        slot_total, D
    )
    picked = (
        jnp.take(returned_rows, targets.reshape(-1), axis=0)
        .reshape(tok_count, TOPK, D)
        .astype(jnp.float32)
    )
    moe_sum = jnp.sum(picked * route_weights[:, :, None], axis=1)
    return (middle + moe_sum).astype(jnp.bfloat16)


def solution(mesh):
    return jax.shard_map(
        shards,
        mesh=mesh,
        in_specs=(
            P("sp", "tp"),
            P("sp", None),
            P("sp", None),
            P(),
            P(None, "tp"),
            P(None, "tp"),
            P(),
            P(),
            P(),
            P(),
            P(("sp", "tp"), None),
            P(),
            P(("sp", "tp"), None),
            P(("sp", "tp"), None),
            P("sp", None, "tp"),
            P("sp", None, "tp"),
            P("sp", "tp", None),
        ),
        out_specs=P(("sp", "tp"), None),
        check_vma=False,
    )
```

profile of v0, /device:TPU:97, one launch (start us, length us, event | category | flops | bytes accessed | tf_op | source)
XLA Modules:
  0.0 451.1 jit_solution(6509418621641927697)
XLA Ops:
  6.6 1.6 fusion.21
  8.3 1.8 fusion.29
  10.1 0.9 fusion.40
  11.0 1.0 fusion.42
  12.0 1.0 fusion.41
  13.0 0.6 fusion.30
  13.7 0.3 fusion.74
  14.1 0.7 pad_maximum_fusion
  14.9 0.2 copy.34
  15.2 0.1 reshape.499
  15.5 0.2 reduce_window_sum.11
  15.7 0.2 select_reduce_fusion
  15.8 0.1 reduce_sum.105
  16.1 61.9 %all-gather.3.cloned.1.call-done = bf16[1,160,16384]{2,1,0:T(8,128)(2,1)} async-done(((bf16[1,160,1024]{2,1,0:T(8,128)(2,1)}), bf16[1,160,16384]{2,1,0:T(8,128)(2,1)}) %all-gather.3.cloned.1.call-update) | async-done | bytes 5242896 | tf_op jit(solution)/shard_map/all_gather | solution.py:114
  78.0 9.9 %while.18 = (s32[]{:T(128)}, f32[1,1024]{1,0:T(1,128)S(1)}, f32[1,1024]{1,0:T(1,128)S(1)}, f32[1,1024,64]{1,2,0:T(8,128)S(1)}, s32[]{:T(128)}, /*index=5*/bf16[1...) while((s32[]{:T(128)}, f32[1,1024]{1,0:T(1,128)S(1)}, ...), condition=%wide.region_8.9_spmd.clone, body=%wide.region_3.8_spmd.clone.sunk | while | flops 352456704 | bytes 30515560 | solution.py:149
  78.0 9.1 %conditional.3 = ((f32[1,1024]{1,0:T(1,128)S(1)}, f32[1,1024]{1,0:T(1,128)S(1)}, f32[1,1024,64]{1,2,0:T(8,128)S(1)})) conditional(s32[]{:T(128)} %convert_element_type.207, (f32[1,1024]{1,0:T(1,128)S(1)}, f32[1,1024]{1,0:T(1,128)S(1)}, f32[1,1024,64]{1,2,0:T(8,128)S(1)}) %tuple.54, (s32[]{:T(128)}, s32[]{:T(128)}, s32[]{:T(128)}, ...), branch_computations={%region_4.0_spmd, %region_5.7_spmd} | conditional | flops 352456704 | bytes 30511242 | solution.py:147
  78.0 2.0 fusion.2
  80.1 2.0 copy-done.1
  82.1 1.5 fusion.4
  83.7 3.5 fusion.10
  87.9 0.2 copy.41
  88.1 0.9 reshape.512
  89.0 7.8 %all-to-all-start = ((bf16[16,2,2048]{2,1,0:T(2,128)(2,1)}), bf16[16,2,2048]{2,1,0:T(2,128)(2,1)S(1)}, u32[]{:S(2)}, u32[]{:S(2)}) async-start(bf16[16,2,2048]{2,1,0:T(2,128)(2,1)} %reshape.512), calls=%async_computation | async-start | bytes 262144 | tf_op jit(solution)/shard_map/all_to_all | solution.py:153
  96.9 6.2 %all-to-all-done = bf16[16,2,2048]{2,1,0:T(2,128)(2,1)S(1)} async-done(((bf16[16,2,2048]{2,1,0:T(2,128)(2,1)}), bf16[16,2,2048]{2,1,0:T(2,128)(2,1)S(1)}, u32[]{:S(2)}, u32[]{:S(2)}) %all-to-all-start) | async-done | bytes 131104 | tf_op jit(solution)/shard_map/all_to_all | solution.py:153
  103.1 0.2 reshape.513
  103.3 0.2 fusion.32
  103.5 3.5 convert_bitcast_fusion
  107.1 0.8 convert_reduce_fusion
  107.8 0.2 copy-done.2
  108.0 0.2 multiply_reduce_fusion.1
  108.2 0.4 convolution_convert_fusion.1
  108.5 0.2 reshape.500
  108.8 156.9 %all_to_all.23 = bf16[16,9,2048]{2,1,0:T(8,128)(2,1)S(1)} all-to-all(bf16[16,9,2048]{2,1,0:T(8,128)(2,1)S(1)} %reshape.500), channel_id=1, replica_groups=mesh['sp'=16,'tp'=16] {'sp'}, dimensions={0} | all-to-all | bytes 1179648 | tf_op jit(solution)/shard_map/all_to_all | solution.py:176
  265.7 1.1 reshape.501
  266.8 0.2 reduce-scatter.2.cloned.1.call-start
  267.1 57.2 %all-gather.5.cloned.1.call-done = bf16[2304,2048]{1,0:T(8,128)(2,1)} async-done(((bf16[144,2048]{1,0:T(8,128)(2,1)}), bf16[2304,2048]{1,0:T(8,128)(2,1)}) %all-gather.5.cloned.1.call-update) | async-done | bytes 9437200 | tf_op jit(solution)/shard_map/all_gather | solution.py:179
  324.3 5.3 %fusion.38 = f32[2304,128]{1,0:T(8,128)S(1)} fusion(bf16[2304,2048]{1,0:T(8,128)(2,1)} %all-gather.5.cloned.1.call-done, bf16[1,2048,128]{2,1,0:T(8,128)(2,1)} %param.35), kind=kOutput, calls=%fused_computation.53 | convolution fusion | flops 1207959552 | bytes 11141120 | tf_op jit(solution)/shard_map/dot_general | solution.py:180
  329.6 14.2 %convolution_convert_fusion = bf16[2304,2048]{1,0:T(8,128)(2,1)} fusion(bf16[2304,2048]{1,0:T(8,128)(2,1)} %all-gather.5.cloned.1.call-done, f32[2304,128]{1,0:T(8,128)S(1)} %fusion.38, bf16[1,128,2048]{2,1,0:T(8,128)(2,1)S(1)} %copy-done, bf16[1,2048,128]{2,1,0:T(8,128)(2,1)S(1)} %copy-done.5), kind=kOutput, calls=%fused_computation.23 | convolution fusion | flops 2422407168 | bytes 21102592 | tf_op jit(solution)/shard_map/dot_general | solution.py:184
  343.9 71.6 %reduce-scatter.2.cloned.1.call-done = bf16[144,2048]{1,0:T(8,128)(2,1)} async-done(((bf16[2304,2048]{1,0:T(8,128)(2,1)}), bf16[144,2048]{1,0:T(8,128)(2,1)}) %reduce-scatter.2.cloned.1.call-update) | async-done | bytes 589840 | tf_op jit(solution)/shard_map/reduce_scatter | solution.py:183
  415.5 2.3 reshape.502
  417.8 6.5 %all-to-all-start.2 = ((bf16[16,9,2048]{2,1,0:T(8,128)(2,1)}), bf16[16,9,2048]{2,1,0:T(8,128)(2,1)S(1)}, u32[]{:S(2)}, u32[]{:S(2)}) async-start(bf16[16,9,2048]{2,1,0:T(8,128)(2,1)} %reshape.502), calls=%async_computation.3 | async-start | bytes 2097152 | tf_op jit(solution)/shard_map/all_to_all | solution.py:189
  424.4 0.1 mul.304
  424.8 15.1 %all-to-all-done.2 = bf16[16,9,2048]{2,1,0:T(8,128)(2,1)S(1)} async-done(((bf16[16,9,2048]{2,1,0:T(8,128)(2,1)}), bf16[16,9,2048]{2,1,0:T(8,128)(2,1)S(1)}, u32[]{:S(2)}, u32[]{:S(2)}) %all-to-all-start.2) | async-done | bytes 589856 | tf_op jit(solution)/shard_map/all_to_all | solution.py:189
  439.9 0.3 reshape.503
  440.2 0.9 gather_fusion
  441.1 0.3 gather.7
  441.4 2.3 multiply_reduce_fusion
  443.8 0.8 add_convert_fusion
  (92 shorter events, 1.4 us)
Async XLA Ops:
  6.5 323.1 %copy-start = (bf16[1,128,2048]{2,1,0:T(8,128)(2,1)S(1)}, bf16[1,128,2048]{2,1,0:T(8,128)(2,1)}, u32[]{:S(2)}) copy-start(bf16[1,128,2048]{2,1,0:T(8,128)(2,1)} %param.37) | copy-start | bytes 1572868
  6.5 6.4 %copy-start.3 = (bf16[1024,512]{1,0:T(8,128)(2,1)S(1)}, bf16[1024,512]{1,0:T(8,128)(2,1)}, u32[]{:S(2)}) copy-start(bf16[1024,512]{1,0:T(8,128)(2,1)} %param.22) | copy-start | bytes 3145732
  6.5 6.5 %copy-start.12 = (f32[512]{0:T(512)S(1)}, f32[512]{0:T(512)}, u32[]{:S(2)}) copy-start(f32[512]{0:T(512)} %param.24) | copy-start | bytes 6148
  6.5 7.0 %copy-start.4 = (bf16[1024,96]{0,1:T(8,128)(2,1)S(1)}, bf16[1024,96]{0,1:T(8,128)(2,1)}, u32[]{:S(2)}) copy-start(bf16[1024,96]{0,1:T(8,128)(2,1)} %param.21) | copy-start | bytes 589828
  6.5 6.5 %copy-start.11 = (bf16[512,64]{0,1:T(8,128)(2,1)S(1)}, bf16[512,64]{0,1:T(8,128)(2,1)}, u32[]{:S(2)}) copy-start(bf16[512,64]{0,1:T(8,128)(2,1)} %param.26) | copy-start | bytes 196612
  6.5 7.0 %copy-start.10 = (f32[96]{0:T(128)S(1)}, f32[96]{0:T(128)}, u32[]{:S(2)}) copy-start(f32[96]{0:T(128)} %param.27) | copy-start | bytes 1156
  6.6 71.4 %all-gather.3.cloned.1.call-start = ((), (), s32[]{:S(2)}) async-start(), calls=%async_computation.4 | async-start | bytes 5570560 | tf_op jit(solution)/shard_map/all_gather | solution.py:114
  8.3 6.8 %copy-start.8 = (f32[1024]{0:T(1024)S(1)}, f32[1024]{0:T(1024)}, u32[]{:S(2)}) copy-start(f32[1024]{0:T(1024)} %param.29) | copy-start | bytes 12292
  8.3 6.9 %copy-start.6 = (s32[64,2]{0,1:T(2,128)S(1)}, s32[64,2]{0,1:T(2,128)}, u32[]{:S(2)}) copy-start(s32[64,2]{0,1:T(2,128)} %param.33) | copy-start | bytes 1540
  80.1 2.0 copy-start.1
  89.0 14.1 %all-to-all-start = ((bf16[16,2,2048]{2,1,0:T(2,128)(2,1)}), bf16[16,2,2048]{2,1,0:T(2,128)(2,1)S(1)}, u32[]{:S(2)}, u32[]{:S(2)}) async-start(bf16[16,2,2048]{2,1,0:T(2,128)(2,1)} %reshape.512), calls=%async_computation | async-start | bytes 262144 | tf_op jit(solution)/shard_map/all_to_all | solution.py:153
  96.8 227.5 %all-gather.5.cloned.1.call-start = ((), (), s32[]{:S(2)}) async-start(), calls=%async_computation.5 | async-start | bytes 10027008 | tf_op jit(solution)/shard_map/all_gather | solution.py:179
  107.0 1.0 copy-start.2
  107.0 1.1 copy-start.7
  266.8 62.8 %copy-start.5 = (bf16[1,2048,128]{2,1,0:T(8,128)(2,1)S(1)}, bf16[1,2048,128]{2,1,0:T(8,128)(2,1)}, u32[]{:S(2)}) copy-start(bf16[1,2048,128]{2,1,0:T(8,128)(2,1)} %param.36) | copy-start | bytes 1572868
  266.8 148.7 %reduce-scatter.2.cloned.1.call-start = ((), (), s32[]{:S(2)}) async-start(), calls=%async_computation.6 | async-start | bytes 10027008 | tf_op jit(solution)/shard_map/reduce_scatter | solution.py:183
  343.8 80.8 %copy-start.9 = (f32[64,2]{0,1:T(2,128)S(1)}, f32[64,2]{0,1:T(2,128)}, u32[]{:S(2)}) copy-start(f32[64,2]{0,1:T(2,128)} %param.34) | copy-start | bytes 1540
  417.8 22.1 %all-to-all-start.2 = ((bf16[16,9,2048]{2,1,0:T(8,128)(2,1)}), bf16[16,9,2048]{2,1,0:T(8,128)(2,1)S(1)}, u32[]{:S(2)}, u32[]{:S(2)}) async-start(bf16[16,9,2048]{2,1,0:T(8,128)(2,1)} %reshape.502), calls=%async_computation.3 | async-start | bytes 2097152 | tf_op jit(solution)/shard_map/all_to_all | solution.py:189
Sparse Core Ops, SparseCore 0:
  14.9 62.9 all-gather.2
  266.9 57.2 all-gather.4
  344.0 71.4 reduce-scatter.1
where the time goes:
time: 452 us; the launch traced here: 451 us
  waiting for transfers between devices  212 us (47%)
  blocking collectives  157 us (35%)
  matrix products  31.3 us (7%)
  starting transfers between devices  14.6 us (3%)
  between operations  13.5 us (3%)
  other arithmetic  12 us (3%)
  local copies, waits for them, and re-layouts  9.85 us (2%)
    all_to_all x1, blocking collectives, shards(): lax.all_to_all(outbound, 'sp', split_axis=0, concat_axis=0, tiled=True)  157 us
    reduce_scatter x1, waiting for transfers between devices, shards(): lax.psum_scatter(jnp.dot(hidden, expert_down[0], preferred_element_type=j...  71.6 us
    all_gather x1, waiting for transfers between devices, shards(): key_piece = lax.all_gather(bundle, 'sp', axis=2, tiled=True)  61.9 us
    all_gather x1, waiting for transfers between devices, shards(): row_block = lax.all_gather(flat_rows, 'tp', axis=0, tiled=True)  57.2 us
    all_to_all x1, waiting for transfers between devices, shards(): lax.all_to_all(served, 'sp', split_axis=0, concat_axis=0, tiled=True)  15.1 us
    dot_general x1, matrix products, shards(): jnp.dot(hidden, expert_down[0], preferred_element_type=jnp.float32)  14.2 us
  transfers between devices with their start and end apart: 5, of which 5 were waited for; matrix products, arithmetic and copies ran while one was open for 0% of the time, Pallas kernels for 0%

commit v1 on v0

--- a/solution.py
+++ b/solution.py
@@ -176,7 +176,9 @@
     arrived = lax.all_to_all(outbound, "sp", split_axis=0, concat_axis=0, tiled=True)
     item_count = arrived.shape[1]
     flat_rows = arrived.reshape(sp_count * item_count, D)
-    row_block = lax.all_gather(flat_rows, "tp", axis=0, tiled=True)
+    row_block = jnp.concatenate(
+        lax.all_to_all(jnp.stack([flat_rows] * lax.axis_size("tp")), "tp", 0, 0), axis=0
+    )
     gate_pre = jnp.dot(row_block, expert_gate[0], preferred_element_type=jnp.float32)
     up_pre = jnp.dot(row_block, expert_up[0], preferred_element_type=jnp.float32)
     hidden = (jax.nn.silu(gate_pre) * up_pre).astype(jnp.bfloat16)

time: 452 us -> 606 us (1.34)
  blocking collectives: 157 us -> 370 us
  waiting for transfers between devices: 212 us -> 151 us
    all_to_all x0 -> x1, blocking collectives: none -> 213 us  [shards(): lax.all_to_all(jnp.stack([flat_rows] * lax.axis_size('tp')), 'tp', 0, 0)]
    all_gather x1 -> x0, waiting for transfers between devices: 57.2 us -> none  [shards(): row_block = lax.all_gather(flat_rows, 'tp', axis=0, tiled=True)]
  transfers between devices with their start and end apart: 5 -> 4, of which waited for: 5 -> 4; matrix products, arithmetic and copies ran while one was open for 0% -> 0% of each run, Pallas kernels for 0% -> 0%
where the time goes in v1:
time: 606 us; the launch traced here: 605 us
  blocking collectives  370 us (61%)
  waiting for transfers between devices  151 us (25%)
  matrix products  28.7 us (5%)
  starting transfers between devices  14.3 us (2%)
  local copies, waits for them, and re-layouts  13.9 us (2%)
  between operations  13.8 us (2%)
  other arithmetic  12 us (2%)
    all_to_all x1, blocking collectives, shards(): lax.all_to_all(jnp.stack([flat_rows] * lax.axis_size('tp')), 'tp', 0, 0)  213 us
    all_to_all x1, blocking collectives, shards(): lax.all_to_all(outbound, 'sp', split_axis=0, concat_axis=0, tiled=True)  157 us
    reduce_scatter x1, waiting for transfers between devices, shards(): lax.psum_scatter(jnp.dot(hidden, expert_down[0], preferred_element_type=j...  68.1 us
    all_gather x1, waiting for transfers between devices, shards(): key_piece = lax.all_gather(bundle, 'sp', axis=2, tiled=True)  61.9 us
    all_to_all x1, waiting for transfers between devices, shards(): lax.all_to_all(served, 'sp', split_axis=0, concat_axis=0, tiled=True)  15.1 us
    dot_general x1, matrix products, shards(): jnp.dot(hidden, expert_down[0], preferred_element_type=jnp.float32)  14.3 us
  transfers between devices with their start and end apart: 4, of which 4 were waited for; matrix products, arithmetic and copies ran while one was open for 0% of the time, Pallas kernels for 0%

profile of v1, /device:TPU:97, one launch (start us, length us, event | category | flops | bytes accessed | tf_op | source)
XLA Modules:
  0.0 604.8 jit_solution(11549392763498200258)
XLA Ops:
  6.6 1.6 fusion.21
  8.3 1.8 fusion.29
  10.1 0.9 fusion.40
  11.0 1.0 fusion.42
  12.0 1.0 fusion.41
  13.0 0.6 fusion.30
  13.7 0.3 fusion.74
  14.1 0.7 pad_maximum_fusion
  14.9 0.2 copy.34
  15.2 0.1 reshape.501
  15.5 0.2 reduce_window_sum.11
  15.7 0.2 select_reduce_fusion
  15.8 0.1 reduce_sum.105
  16.1 61.9 %all-gather.2.cloned.1.call-done = bf16[1,160,16384]{2,1,0:T(8,128)(2,1)} async-done(((bf16[1,160,1024]{2,1,0:T(8,128)(2,1)}), bf16[1,160,16384]{2,1,0:T(8,128)(2,1)}) %all-gather.2.cloned.1.call-update) | async-done | bytes 5242896 | tf_op jit(solution)/shard_map/all_gather | solution.py:114
  78.0 9.9 %while.18 = (s32[]{:T(128)}, f32[1,1024]{1,0:T(1,128)S(1)}, f32[1,1024]{1,0:T(1,128)S(1)}, f32[1,1024,64]{1,2,0:T(8,128)S(1)}, s32[]{:T(128)}, /*index=5*/bf16[1...) while((s32[]{:T(128)}, f32[1,1024]{1,0:T(1,128)S(1)}, ...), condition=%wide.region_8.9_spmd.clone, body=%wide.region_3.8_spmd.clone.sunk | while | flops 352456704 | bytes 30515560 | solution.py:149
  78.0 9.1 %conditional.3 = ((f32[1,1024]{1,0:T(1,128)S(1)}, f32[1,1024]{1,0:T(1,128)S(1)}, f32[1,1024,64]{1,2,0:T(8,128)S(1)})) conditional(s32[]{:T(128)} %convert_element_type.207, (f32[1,1024]{1,0:T(1,128)S(1)}, f32[1,1024]{1,0:T(1,128)S(1)}, f32[1,1024,64]{1,2,0:T(8,128)S(1)}) %tuple.54, (s32[]{:T(128)}, s32[]{:T(128)}, s32[]{:T(128)}, ...), branch_computations={%region_4.0_spmd, %region_5.7_spmd} | conditional | flops 352456704 | bytes 30511242 | solution.py:147
  78.0 2.0 fusion.2
  80.1 2.0 copy-done.1
  82.1 1.5 fusion.4
  83.7 3.5 fusion.10
  87.9 0.2 copy.41
  88.1 0.9 reshape.514
  89.0 7.8 %all-to-all-start = ((bf16[16,2,2048]{2,1,0:T(2,128)(2,1)}), bf16[16,2,2048]{2,1,0:T(2,128)(2,1)S(1)}, u32[]{:S(2)}, u32[]{:S(2)}) async-start(bf16[16,2,2048]{2,1,0:T(2,128)(2,1)} %reshape.514), calls=%async_computation | async-start | bytes 262144 | tf_op jit(solution)/shard_map/all_to_all | solution.py:153
  96.9 6.2 %all-to-all-done = bf16[16,2,2048]{2,1,0:T(2,128)(2,1)S(1)} async-done(((bf16[16,2,2048]{2,1,0:T(2,128)(2,1)}), bf16[16,2,2048]{2,1,0:T(2,128)(2,1)S(1)}, u32[]{:S(2)}, u32[]{:S(2)}) %all-to-all-start) | async-done | bytes 131104 | tf_op jit(solution)/shard_map/all_to_all | solution.py:153
  103.1 0.2 reshape.515
  103.3 0.2 fusion.32
  103.5 3.5 convert_bitcast_fusion
  107.1 0.8 convert_reduce_fusion
  107.8 0.2 copy-done.3
  108.0 0.2 multiply_reduce_fusion.1
  108.2 0.4 convolution_convert_fusion.1
  108.5 0.2 reshape.502
  108.8 156.9 %all_to_all.28 = bf16[16,9,2048]{2,1,0:T(8,128)(2,1)S(1)} all-to-all(bf16[16,9,2048]{2,1,0:T(8,128)(2,1)S(1)} %reshape.502), channel_id=1, replica_groups=mesh['sp'=16,'tp'=16] {'sp'}, dimensions={0} | all-to-all | bytes 1179648 | tf_op jit(solution)/shard_map/all_to_all | solution.py:176
  265.7 0.3 stack_reshape.2
  266.0 1.2 stack.3
  267.2 213.0 %all_to_all.29 = bf16[16,144,2048]{2,1,0:T(8,128)(2,1)S(1)} all-to-all(bf16[16,144,2048]{2,1,0:T(8,128)(2,1)S(1)} %stack.3), channel_id=1, replica_groups=mesh['sp'=16,'tp'=16] {'tp'}, dimensions={0} | all-to-all | bytes 18874368 | tf_op jit(solution)/shard_map/all_to_all | solution.py:180
  480.2 3.7 copy-done.2
  483.8 2.7 fusion.38
  486.5 14.3 %convolution_convert_fusion = bf16[2304,2048]{1,0:T(8,128)(2,1)} fusion(bf16[2304,2048]{1,0:T(8,128)(2,1)} %bitcast.85, f32[2304,128]{1,0:T(8,128)S(1)} %fusion.38, bf16[1,128,2048]{2,1,0:T(8,128)(2,1)S(1)} %copy-done, bf16[1,2048,128]{2,1,0:T(8,128)(2,1)S(1)} %copy-done.6), kind=kOutput, calls=%fused_computation.23 | convolution fusion | flops 2422407168 | bytes 21102592 | tf_op jit(solution)/shard_map/dot_general | solution.py:186
  500.8 68.1 %reduce-scatter.2.cloned.1.call-done = bf16[144,2048]{1,0:T(8,128)(2,1)} async-done(((bf16[2304,2048]{1,0:T(8,128)(2,1)}), bf16[144,2048]{1,0:T(8,128)(2,1)}) %reduce-scatter.2.cloned.1.call-update) | async-done | bytes 589840 | tf_op jit(solution)/shard_map/reduce_scatter | solution.py:185
  568.9 2.3 reshape.504
  571.2 6.5 %all-to-all-start.3 = ((bf16[16,9,2048]{2,1,0:T(8,128)(2,1)}), bf16[16,9,2048]{2,1,0:T(8,128)(2,1)S(1)}, u32[]{:S(2)}, u32[]{:S(2)}) async-start(bf16[16,9,2048]{2,1,0:T(8,128)(2,1)} %reshape.504), calls=%async_computation.4 | async-start | bytes 2097152 | tf_op jit(solution)/shard_map/all_to_all | solution.py:191
  578.2 15.1 %all-to-all-done.3 = bf16[16,9,2048]{2,1,0:T(8,128)(2,1)S(1)} async-done(((bf16[16,9,2048]{2,1,0:T(8,128)(2,1)}), bf16[16,9,2048]{2,1,0:T(8,128)(2,1)S(1)}, u32[]{:S(2)}, u32[]{:S(2)}) %all-to-all-start.3) | async-done | bytes 589856 | tf_op jit(solution)/shard_map/all_to_all | solution.py:191
  593.3 0.3 reshape.505
  593.5 0.9 gather_fusion
  594.5 0.3 gather.7
  594.8 2.3 multiply_reduce_fusion
  597.1 0.8 add_convert_fusion
  (95 shorter events, 1.6 us)
Async XLA Ops:
  6.5 480.0 %copy-start = (bf16[1,128,2048]{2,1,0:T(8,128)(2,1)S(1)}, bf16[1,128,2048]{2,1,0:T(8,128)(2,1)}, u32[]{:S(2)}) copy-start(bf16[1,128,2048]{2,1,0:T(8,128)(2,1)} %param.37) | copy-start | bytes 1572868
  6.5 6.4 %copy-start.4 = (bf16[1024,512]{1,0:T(8,128)(2,1)S(1)}, bf16[1024,512]{1,0:T(8,128)(2,1)}, u32[]{:S(2)}) copy-start(bf16[1024,512]{1,0:T(8,128)(2,1)} %param.22) | copy-start | bytes 3145732
  6.5 6.5 %copy-start.14 = (f32[512]{0:T(512)S(1)}, f32[512]{0:T(512)}, u32[]{:S(2)}) copy-start(f32[512]{0:T(512)} %param.24) | copy-start | bytes 6148
  6.5 7.0 %copy-start.5 = (bf16[1024,96]{0,1:T(8,128)(2,1)S(1)}, bf16[1024,96]{0,1:T(8,128)(2,1)}, u32[]{:S(2)}) copy-start(bf16[1024,96]{0,1:T(8,128)(2,1)} %param.21) | copy-start | bytes 589828
  6.5 6.5 %copy-start.13 = (bf16[512,64]{0,1:T(8,128)(2,1)S(1)}, bf16[512,64]{0,1:T(8,128)(2,1)}, u32[]{:S(2)}) copy-start(bf16[512,64]{0,1:T(8,128)(2,1)} %param.26) | copy-start | bytes 196612
  6.5 7.0 %copy-start.11 = (f32[96]{0:T(128)S(1)}, f32[96]{0:T(128)}, u32[]{:S(2)}) copy-start(f32[96]{0:T(128)} %param.27) | copy-start | bytes 1156
  6.6 71.4 %all-gather.2.cloned.1.call-start = ((), (), s32[]{:S(2)}) async-start(), calls=%async_computation.5 | async-start | bytes 5570560 | tf_op jit(solution)/shard_map/all_gather | solution.py:114
  8.3 6.8 %copy-start.9 = (f32[1024]{0:T(1024)S(1)}, f32[1024]{0:T(1024)}, u32[]{:S(2)}) copy-start(f32[1024]{0:T(1024)} %param.29) | copy-start | bytes 12292
  8.3 6.9 %copy-start.7 = (s32[64,2]{0,1:T(2,128)S(1)}, s32[64,2]{0,1:T(2,128)}, u32[]{:S(2)}) copy-start(s32[64,2]{0,1:T(2,128)} %param.33) | copy-start | bytes 1540
  80.1 2.0 copy-start.1
  89.0 14.1 %all-to-all-start = ((bf16[16,2,2048]{2,1,0:T(2,128)(2,1)}), bf16[16,2,2048]{2,1,0:T(2,128)(2,1)S(1)}, u32[]{:S(2)}, u32[]{:S(2)}) async-start(bf16[16,2,2048]{2,1,0:T(2,128)(2,1)} %reshape.514), calls=%async_computation | async-start | bytes 262144 | tf_op jit(solution)/shard_map/all_to_all | solution.py:153
  96.8 472.1 %reduce-scatter.2.cloned.1.call-start = ((), (), s32[]{:S(2)}) async-start(), calls=%async_computation.6 | async-start | bytes 10027008 | tf_op jit(solution)/shard_map/reduce_scatter | solution.py:185
  107.0 1.0 copy-start.3
  107.0 1.1 copy-start.8
  267.2 216.6 %copy-start.12 = (bf16[1,2048,128]{2,1,0:T(8,128)(2,1)S(1)}, bf16[1,2048,128]{2,1,0:T(8,128)(2,1)}, u32[]{:S(2)}) copy-start(bf16[1,2048,128]{2,1,0:T(8,128)(2,1)} %param.35) | copy-start | bytes 1572868
  480.2 3.7 copy-start.2
  483.8 2.7 copy-start.6
  500.8 77.3 %copy-start.10 = (f32[64,2]{0,1:T(2,128)S(1)}, f32[64,2]{0,1:T(2,128)}, u32[]{:S(2)}) copy-start(f32[64,2]{0,1:T(2,128)} %param.34) | copy-start | bytes 1540
  571.2 22.1 %all-to-all-start.3 = ((bf16[16,9,2048]{2,1,0:T(8,128)(2,1)}), bf16[16,9,2048]{2,1,0:T(8,128)(2,1)S(1)}, u32[]{:S(2)}, u32[]{:S(2)}) async-start(bf16[16,9,2048]{2,1,0:T(8,128)(2,1)} %reshape.504), calls=%async_computation.4 | async-start | bytes 2097152 | tf_op jit(solution)/shard_map/all_to_all | solution.py:191
Sparse Core Ops, SparseCore 0:
  14.9 62.9 all-gather.1
  500.9 67.9 reduce-scatter.1
